TPU v7x, 32 devices: a whole 2x2x4 slice. The times are simulated.
32 devices in a mesh: ep: 8 (over z, core), tp: 4 (over y, x).
Axes of the slice: x: 2, y: 2, z: 4, core: 2. Of those that a mesh axis runs over, the one named last changes fastest.
Arguments:
- resid: bfloat16 [32, 2048], P('ep', 'tp'), may hold values from -6 to 6
- cache_key: bfloat16 [32, 8, 224, 256], P(('ep', 'tp')), may hold values from -360 to 360
- cache_value: bfloat16 [32, 8, 224, 256], P(('ep', 'tp')), may hold values from -6 to 6
- lengths: int32 [32], P(('ep', 'tp')), may hold values from 28 to 224
- lambdas: float32 [8], replicated, may hold values from 0.3 to 0.8
- mix_gain: float32 [2048], replicated, may hold values from 0.1 to 1.9
- query_gain: float32 [128], replicated, may hold values from 0.1 to 1.9
- key_gain: float32 [128], replicated, may hold values from 0.1 to 1.9
- sub_gain: float32 [256], replicated, may hold values from 0.1 to 1.9
- ffn_gain: float32 [2048], replicated, may hold values from 0.1 to 1.9
- w_query: bfloat16 [2048, 2048], P(None, 'tp'), may hold values from -0.125 to 0.125
- w_key: bfloat16 [2048, 2048], P(None, 'tp'), may hold values from -0.125 to 0.125
- w_value: bfloat16 [2048, 2048], P(None, 'tp'), may hold values from -0.125 to 0.125
- w_out: bfloat16 [2048, 2048], P(None, 'tp'), may hold values from -0.125 to 0.125
- routes: int32 [32, 2], P('ep'), may hold values from 0 to 7, all different within a row; in each aligned block of 4 rows (0 to 3, 4 to 7, ...) at most 4 rows name the same one
- route_weights: float32 [32, 2], P('ep'), may hold values from 0.2 to 0.8
- w_gate: bfloat16 [8, 2048, 4096], P('ep', None, 'tp'), may hold values from -0.125 to 0.125
- w_up: bfloat16 [8, 2048, 4096], P('ep', None, 'tp'), may hold values from -0.125 to 0.125
- w_down: bfloat16 [8, 4096, 2048], P('ep', 'tp'), may hold values from -0.09375 to 0.09375
Outputs:
- result: bfloat16 [32, 2048], P('ep', 'tp')
- new_key: bfloat16 [32, 8, 256], P(('ep', 'tp'))
- new_value: bfloat16 [32, 8, 256], P(('ep', 'tp'))
Inputs may be any that keep to these rules, and one draw needn't show every extreme that they name: `routes`: within the 4 rows of one index of ep no expert is named more than 4 times, and in some of them one expert is named exactly 4 times; the two experts of a row differ. `lengths`: every sequence has at least two live positions.
All inputs are finite; a program needn't handle non-finite values.
Results may differ from a plain program's by a relative error of at most 0.0099.
Values may be sent and summed in bfloat16 or wider, within the bound.
A program may use at most 64 MiB of HBM per device.

v0:
```python
import math
import jax
import jax.numpy as jnp
from jax import lax
from jax.sharding import PartitionSpec as P

CAP = 4
epsilon = 1e-06
out_factor = 0.2 + 0.6 * math.exp(-0.3)
masked_score = -1e30


def scaled_rows(values, gain):
    wide = values.astype(jnp.float32)
    return wide * lax.rsqrt(jnp.mean(wide * wide, axis=-1, keepdims=True) + epsilon) * gain


def route_tables(routes, route_weights, experts, capacity):
    flat_routes = routes.reshape(-1)
    expert_hit = (flat_routes[:, None] == jnp.arange(experts, dtype=jnp.int32)[None, :]).astype(
        jnp.int32
    )
    before = jnp.cumsum(expert_hit, axis=0) - expert_hit
    slot_index = jnp.sum(before * expert_hit, axis=1)
    slot_hit = (slot_index[:, None] == jnp.arange(capacity, dtype=jnp.int32)[None, :]).astype(
        jnp.float32
    )
    pair_table = expert_hit.astype(jnp.float32)[:, :, None] * slot_hit[:, None, :]
    pair_table = pair_table.reshape(routes.shape[0], 2, experts, capacity)
    dispatch = jnp.sum(pair_table, axis=1)
    combine = jnp.sum(pair_table * route_weights[:, :, None, None], axis=1)
    return (dispatch, combine)


def attend(
    queries,
    key_rows,
    value_rows,
    past_keys,
    past_values,
    live_len,
    lambdas,
    query_gain,
    key_gain,
    sub_gain,
):
    seq_count, kv_heads, cache_len, key_width = past_keys.shape
    head_dim = key_width // 2
    head_count = lambdas.shape[0]
    group_size = head_count // kv_heads
    value_dim = past_values.shape[-1]
    score_scale = head_dim ** (-0.5)
    q_unit = scaled_rows(
        queries.reshape(seq_count, kv_heads, group_size, 2, head_dim), query_gain
    ).astype(jnp.bfloat16)
    new_key = scaled_rows(key_rows.reshape(seq_count, kv_heads, 2, head_dim), key_gain).astype(
        jnp.bfloat16
    )
    new_value = value_rows.reshape(seq_count, kv_heads, value_dim)
    past_split = past_keys.reshape(seq_count, kv_heads, cache_len, 2, head_dim)
    scores = (
        jnp.einsum("sjgmd,sjlmd->sjgml", q_unit, past_split, preferred_element_type=jnp.float32)
        * score_scale
    )
    own_score = (
        jnp.einsum("sjgmd,sjmd->sjgm", q_unit, new_key, preferred_element_type=jnp.float32)
        * score_scale
    )
    live_mask = jnp.arange(cache_len, dtype=jnp.int32)[None, :] < live_len[:, None]
    scores = jnp.where(live_mask[:, None, None, None, :], scores, masked_score)
    peak = jnp.maximum(jnp.max(scores, axis=-1), own_score)
    past_weight = jnp.exp(scores - peak[..., None])
    own_weight = jnp.exp(own_score - peak)
    totals = jnp.sum(past_weight, axis=-1) + own_weight
    past_prob = past_weight / totals[..., None]
    own_prob = own_weight / totals
    mix_lambda = lambdas.reshape(1, kv_heads, group_size, 1)
    past_mix = (past_prob[..., 0, :] - mix_lambda * past_prob[..., 1, :]).astype(jnp.bfloat16)
    own_mix = (own_prob[..., 0] - mix_lambda[..., 0] * own_prob[..., 1]).astype(jnp.bfloat16)
    head_out = jnp.einsum(
        "sjgl,sjlv->sjgv", past_mix, past_values, preferred_element_type=jnp.float32
    )
    head_out = (
        head_out
        + own_mix.astype(jnp.float32)[..., None] * new_value.astype(jnp.float32)[:, :, None, :]
    )
    mixed = (
        (scaled_rows(head_out, sub_gain) * out_factor)
        .astype(jnp.bfloat16)
        .reshape(seq_count, head_count * value_dim)
    )
    return (mixed, new_key.reshape(seq_count, kv_heads, key_width), new_value)


def local(
    resid,
    cache_key,
    cache_value,
    lengths,
    lambdas,
    mix_gain,
    query_gain,
    key_gain,
    sub_gain,
    ffn_gain,
    w_query,
    w_key,
    w_value,
    w_out,
    routes,
    route_weights,
    w_gate,
    w_up,
    w_down,
):
    gathered = lax.all_gather(resid, "tp", axis=1, tiled=True)
    normed = scaled_rows(gathered, mix_gain).astype(jnp.bfloat16)
    query_part = jnp.dot(normed, w_query, preferred_element_type=jnp.float32).astype(jnp.bfloat16)
    key_part = jnp.dot(normed, w_key, preferred_element_type=jnp.float32).astype(jnp.bfloat16)
    value_part = jnp.dot(normed, w_value, preferred_element_type=jnp.float32).astype(jnp.bfloat16)
    queries, key_rows, value_rows = (
        lax.all_to_all(query_part, "tp", split_axis=0, concat_axis=1, tiled=True),
        lax.all_to_all(key_part, "tp", split_axis=0, concat_axis=1, tiled=True),
        lax.all_to_all(value_part, "tp", split_axis=0, concat_axis=1, tiled=True),
    )
    mixed, new_key, new_value = attend(
        queries,
        key_rows,
        value_rows,
        cache_key,
        cache_value,
        lengths,
        lambdas,
        query_gain,
        key_gain,
        sub_gain,
    )
    attn_proj = jnp.dot(
        lax.all_gather(mixed, "tp", axis=0, tiled=True), w_out, preferred_element_type=jnp.float32
    )
    updated = (resid.astype(jnp.float32) + attn_proj).astype(jnp.bfloat16)
    updated_rows = lax.all_gather(updated, "tp", axis=1, tiled=True)
    hidden = scaled_rows(updated_rows, ffn_gain).astype(jnp.bfloat16)
    experts = w_gate.shape[0] * lax.axis_size("ep")
    dispatch, combine = route_tables(routes, route_weights, experts, CAP)
    send = jnp.einsum(
        "gec,gd->ecd", dispatch.astype(jnp.bfloat16), hidden, preferred_element_type=jnp.float32
    ).astype(jnp.bfloat16)
    slots = lax.all_to_all(send, "ep", split_axis=0, concat_axis=0, tiled=True)
    flat_rows = slots.reshape(-1, slots.shape[-1])
    gate_out = jnp.dot(flat_rows, w_gate[0], preferred_element_type=jnp.float32)
    up_out = jnp.dot(flat_rows, w_up[0], preferred_element_type=jnp.float32)
    act = (jax.nn.silu(gate_out) * up_out).astype(jnp.bfloat16)
    down_out = jnp.dot(act, w_down[0], preferred_element_type=jnp.float32)
    partial_value = down_out.reshape(slots.shape[0], slots.shape[1], down_out.shape[-1])
    flat_combine = combine.reshape(combine.shape[0], -1)
    summed = lax.psum_scatter(
        partial_value.astype(jnp.bfloat16), "tp", scatter_dimension=2, tiled=True
    ).astype(jnp.float32)
    returned = lax.all_to_all(
        summed.astype(jnp.bfloat16), "ep", split_axis=0, concat_axis=0, tiled=True
    ).astype(summed.dtype)
    expert_mix = jnp.dot(
        flat_combine,
        returned.reshape(-1, returned.shape[-1]),
        precision=lax.Precision.HIGHEST,
        preferred_element_type=jnp.float32,
    )
    result = (updated.astype(jnp.float32) + expert_mix).astype(jnp.bfloat16)
    return (result, new_key, new_value)


def solution(mesh):
    in_specs = (
        P("ep", "tp"),
        P(("ep", "tp"), None, None, None),
        P(("ep", "tp"), None, None, None),
        P(("ep", "tp")),
        P(),
        P(),
        P(),
        P(),
        P(),
        P(),
        P(None, "tp"),
        P(None, "tp"),
        P(None, "tp"),
        P(None, "tp"),
        P("ep", None),
        P("ep", None),
        P("ep", None, "tp"),
        P("ep", None, "tp"),
        P("ep", "tp", None),
    )
    out_specs = (P("ep", "tp"), P(("ep", "tp"), None, None), P(("ep", "tp"), None, None))
    return jax.shard_map(local, mesh=mesh, in_specs=in_specs, out_specs=out_specs, check_vma=False)
```

profile of v0, /device:TPU:0, one launch (start us, length us, event | category | flops | bytes accessed | tf_op | source)
XLA Modules:
  0.0 129.9 jit_solution(2296652605895860037)
XLA Ops:
  7.2 9.9 %all_gather.9 = bf16[4,2048]{1,0:T(4,128)(2,1)S(1)} all-gather(bf16[4,512]{1,0:T(4,128)(2,1)} %param.19), channel_id=1, replica_groups=mesh['ep'=8,'tp'=4] {'tp'}, dimensions={1}, use_global_device_ids=true | all-gather | bytes 20480 | tf_op jit(solution)/shard_map/all_gather | solution.py:116
  17.3 1.1 fusion.18
  20.2 3.2 %all-to-all-start = ((bf16[4,2,256]{2,1,0:T(2,128)(2,1)}), bf16[4,2,256]{2,1,0:T(2,128)(2,1)S(1)}, u32[]{:S(2)}, u32[]{:S(2)}) async-start(bf16[4,2,256]{2,1,0:T(2,128)(2,1)} %reshape.382), calls=%async_computation | async-start | bytes 8192 | tf_op jit(solution)/shard_map/all_to_all | solution.py:122
  23.7 2.1 %fusion.19 = bf16[4,1,512]{2,0,1:T(4,128)(2,1)S(1)} fusion(bf16[2048,512]{1,0:T(8,128)(2,1)} %param.30, bf16[4,2048]{1,0:T(4,128)(2,1)S(1)} %all_gather.9, f32[2048]{0:T(1024)S(1)} %copy-done.3, f32[4]{0:T(128)S(1)} %add_rsqrt_fusion.4), kind=kOutput, calls=%fused_computation.19 | convolution fusion | flops 8423424 | bytes 2125840 | tf_op jit(solution)/shard_map/dot_general | solution.py:119
  27.6 0.7 reduce.18
  28.9 2.2 %reshape.356 = bf16[8,224,2,128]{3,2,1,0:T(2,128)(2,1)S(1)} reshape(bf16[1,8,224,256]{3,2,1,0:T(8,128)(2,1)} %param.20) | data formatting | bytes 1835008 | tf_op jit(solution)/shard_map/reshape.7
  31.1 0.7 reduce.17
  32.3 4.2 %all-to-all-start.1 = ((bf16[4,2,256]{2,1,0:T(2,128)(2,1)}), bf16[4,2,256]{2,1,0:T(2,128)(2,1)S(1)}, u32[]{:S(2)}, u32[]{:S(2)}) async-start(bf16[4,2,256]{2,1,0:T(2,128)(2,1)} %reshape.384), calls=%async_computation.1 | async-start | bytes 8192 | tf_op jit(solution)/shard_map/all_to_all | solution.py:123
  36.5 4.6 %all-to-all-done.1 = bf16[4,2,256]{2,1,0:T(2,128)(2,1)S(1)} async-done(((bf16[4,2,256]{2,1,0:T(2,128)(2,1)}), bf16[4,2,256]{2,1,0:T(2,128)(2,1)S(1)}, u32[]{:S(2)}, u32[]{:S(2)}) %all-to-all-start.1) | async-done | bytes 4128 | tf_op jit(solution)/shard_map/all_to_all | solution.py:123
  41.2 3.2 %all-to-all-start.2 = ((bf16[4,2,256]{2,1,0:T(2,128)(2,1)}), bf16[4,2,256]{2,1,0:T(2,128)(2,1)S(1)}, u32[]{:S(2)}, u32[]{:S(2)}) async-start(bf16[4,2,256]{2,1,0:T(2,128)(2,1)} %reshape.380), calls=%async_computation.2 | async-start | bytes 8192 | tf_op jit(solution)/shard_map/all_to_all | solution.py:124
  46.1 3.0 %all-to-all-done.2 = bf16[4,2,256]{2,1,0:T(2,128)(2,1)S(1)} async-done(((bf16[4,2,256]{2,1,0:T(2,128)(2,1)}), bf16[4,2,256]{2,1,0:T(2,128)(2,1)S(1)}, u32[]{:S(2)}, u32[]{:S(2)}) %all-to-all-start.2) | async-done | bytes 4128 | tf_op jit(solution)/shard_map/all_to_all | solution.py:124
  49.1 1.4 %fusion.21 = f32[8,1,256]{2,1,0:T(1,128)S(1)} fusion(bf16[1,8,224,256]{3,2,1,0:T(8,128)(2,1)} %param.21, bf16[8,224,1]{1,0,2:T(8,128)(2,1)S(1)} %fusion.49), kind=kOutput, calls=%fused_computation.21 | convolution fusion | flops 917504 | bytes 929280 | tf_op jit(solution)/shard_map/sjgl,sjlv->sjgv/dot_general | solution.py:80
  50.8 7.2 %all-gather = bf16[4,1,2048]{2,1,0:T(2,128)(2,1)S(1)} all-gather(bf16[1,1,2048]{2,1,0:T(2,128)(2,1)S(1)} %reshape.365), channel_id=1, replica_groups=mesh['ep'=8,'tp'=4] {'tp'}, dimensions={0}, use_global_device_ids=true | all-gather | bytes 20480 | tf_op jit(solution)/shard_map/all_gather | solution.py:139
  58.1 2.0 %fusion.15 = bf16[4,512]{1,0:T(4,128)(2,1)S(1)} fusion(bf16[2048,512]{1,0:T(8,128)(2,1)} %param.32, bf16[4,1,2048]{2,1,0:T(2,128)(2,1)S(1)} %all-gather, bf16[4,512]{1,0:T(4,128)(2,1)S(1)} %copy-done.4), kind=kOutput, calls=%fused_computation.12 | convolution fusion | flops 8394752 | bytes 2121728 | tf_op jit(solution)/shard_map/dot_general | solution.py:138
  60.1 8.1 %all_gather.11 = bf16[4,2048]{1,0:T(4,128)(2,1)S(1)} all-gather(bf16[4,512]{1,0:T(4,128)(2,1)S(1)} %fusion.15), channel_id=1, replica_groups=mesh['ep'=8,'tp'=4] {'tp'}, dimensions={1}, use_global_device_ids=true | all-gather | bytes 20480 | tf_op jit(solution)/shard_map/all_gather | solution.py:142
  68.7 11.4 %all_to_all.49 = bf16[8,4,2048]{2,1,0:T(4,128)(2,1)S(1)} all-to-all(bf16[8,4,2048]{2,1,0:T(4,128)(2,1)S(1)} %copy.68), channel_id=1, replica_groups=mesh['ep'=8,'tp'=4] {'ep'}, dimensions={0} | all-to-all | bytes 262144 | tf_op jit(solution)/shard_map/all_to_all | solution.py:149
  80.2 3.2 %fusion.4 = f32[32,1024]{1,0:T(8,128)S(1)} fusion(bf16[32,2048]{1,0:T(8,128)(2,1)S(1)} %reshape.359, bf16[1,2048,1024]{2,1,0:T(8,128)(2,1)} %param.35), kind=kOutput, calls=%fused_computation.4 | convolution fusion | flops 134217728 | bytes 4456448 | tf_op jit(solution)/shard_map/dot_general | solution.py:151
  83.6 0.8 fusion.12
  84.5 3.6 %fusion.6 = bf16[8,4,2048]{2,0,1:T(8,128)(2,1)} fusion(bf16[1,1024,2048]{2,1,0:T(8,128)(2,1)} %param.37, bf16[8,4,1024]{2,1,0:T(4,128)(2,1)S(1)} %dot_general.48), kind=kOutput, calls=%fused_computation.6 | convolution fusion | flops 134283264 | bytes 4390912 | tf_op jit(solution)/shard_map/dot_general | solution.py:154
  88.3 22.2 %reduce-scatter.2.cloned.1.call-done = bf16[8,4,512]{2,0,1:T(8,128)(2,1)} async-done(((bf16[8,4,2048]{2,0,1:T(8,128)(2,1)}), bf16[8,4,512]{2,0,1:T(8,128)(2,1)}) %reduce-scatter.2.cloned.1.call-update) | async-done | bytes 32784 | tf_op jit(solution)/shard_map/reduce_scatter | solution.py:157
  110.5 1.4 %copy.70 = bf16[8,4,512]{2,1,0:T(4,128)(2,1)} copy(bf16[8,4,512]{2,0,1:T(8,128)(2,1)} %reduce-scatter.2.cloned.1.call-done) | data formatting | bytes 65536 | tf_op jit(solution)/shard_map/reduce_scatter | solution.py:157
  111.9 4.6 %all-to-all-start.4 = ((bf16[8,4,512]{2,1,0:T(4,128)(2,1)}), bf16[8,4,512]{2,1,0:T(4,128)(2,1)S(1)}, u32[]{:S(2)}, u32[]{:S(2)}) async-start(bf16[8,4,512]{2,1,0:T(4,128)(2,1)} %copy.70), calls=%async_computation.5 | async-start | bytes 65536 | tf_op jit(solution)/shard_map/all_to_all | solution.py:160
  117.7 4.5 %all-to-all-done.4 = bf16[8,4,512]{2,1,0:T(4,128)(2,1)S(1)} async-done(((bf16[8,4,512]{2,1,0:T(4,128)(2,1)}), bf16[8,4,512]{2,1,0:T(4,128)(2,1)S(1)}, u32[]{:S(2)}, u32[]{:S(2)}) %all-to-all-start.4) | async-done | bytes 32800 | tf_op jit(solution)/shard_map/all_to_all | solution.py:160
  122.2 0.8 fusion.17
  (86 shorter events, 8.7 us)
Async XLA Ops:
  7.2 10.1 %copy-start = (bf16[2048,512]{1,0:T(8,128)(2,1)S(1)}, bf16[2048,512]{1,0:T(8,128)(2,1)}, u32[]{:S(2)}) copy-start(bf16[2048,512]{1,0:T(8,128)(2,1)} %param.29) | copy-start | bytes 6291460
  7.2 16.5 %copy-start.3 = (f32[2048]{0:T(1024)S(1)}, f32[2048]{0:T(1024)}, u32[]{:S(2)}) copy-start(f32[2048]{0:T(1024)} %param.24) | copy-start | bytes 24580
  7.2 16.2 %copy-start.7 = (s32[4,2]{0,1:T(2,128)S(1)}, s32[4,2]{0,1:T(2,128)}, u32[]{:S(2)}) copy-start(s32[4,2]{0,1:T(2,128)} %param.33) | copy-start | bytes 100
  20.2 12.2 %all-to-all-start = ((bf16[4,2,256]{2,1,0:T(2,128)(2,1)}), bf16[4,2,256]{2,1,0:T(2,128)(2,1)S(1)}, u32[]{:S(2)}, u32[]{:S(2)}) async-start(bf16[4,2,256]{2,1,0:T(2,128)(2,1)} %reshape.382), calls=%async_computation | async-start | bytes 8192 | tf_op jit(solution)/shard_map/all_to_all | solution.py:122
  23.6 2.9 %copy-start.2 = (bf16[2048,512]{1,0:T(8,128)(2,1)S(1)}, bf16[2048,512]{1,0:T(8,128)(2,1)}, u32[]{:S(2)}) copy-start(bf16[2048,512]{1,0:T(8,128)(2,1)} %param.31) | copy-start | bytes 6291460
  23.7 3.7 %copy-start.8 = (f32[4,2]{0,1:T(2,128)S(1)}, f32[4,2]{0,1:T(2,128)}, u32[]{:S(2)}) copy-start(f32[4,2]{0,1:T(2,128)} %param.34) | copy-start | bytes 100
  26.5 18.2 %copy-start.10 = (f32[128]{0:T(128)S(1)}, f32[128]{0:T(128)}, u32[]{:S(2)}) copy-start(f32[128]{0:T(128)} %param.25) | copy-start | bytes 1540
  26.5 18.2 %copy-start.11 = (f32[128]{0:T(128)S(1)}, f32[128]{0:T(128)}, u32[]{:S(2)}) copy-start(f32[128]{0:T(128)} %param.26) | copy-start | bytes 1540
  27.0 19.0 %copy-start.6 = (f32[8]{0:T(128)S(1)}, f32[8]{0:T(128)}, u32[]{:S(2)}) copy-start(f32[8]{0:T(128)} %param.23) | copy-start | bytes 100
  27.0 23.8 %copy-start.9 = (f32[256]{0:T(256)S(1)}, f32[256]{0:T(256)}, u32[]{:S(2)}) copy-start(f32[256]{0:T(256)} %param.27) | copy-start | bytes 3076
  28.9 29.2 %copy-start.4 = (bf16[4,512]{1,0:T(4,128)(2,1)S(1)}, bf16[4,512]{1,0:T(4,128)(2,1)}, u32[]{:S(2)}) copy-start(bf16[4,512]{1,0:T(4,128)(2,1)} %param.19) | copy-start | bytes 12292
  32.3 8.8 %all-to-all-start.1 = ((bf16[4,2,256]{2,1,0:T(2,128)(2,1)}), bf16[4,2,256]{2,1,0:T(2,128)(2,1)S(1)}, u32[]{:S(2)}, u32[]{:S(2)}) async-start(bf16[4,2,256]{2,1,0:T(2,128)(2,1)} %reshape.384), calls=%async_computation.1 | async-start | bytes 8192 | tf_op jit(solution)/shard_map/all_to_all | solution.py:123
  41.2 7.9 %all-to-all-start.2 = ((bf16[4,2,256]{2,1,0:T(2,128)(2,1)}), bf16[4,2,256]{2,1,0:T(2,128)(2,1)S(1)}, u32[]{:S(2)}, u32[]{:S(2)}) async-start(bf16[4,2,256]{2,1,0:T(2,128)(2,1)} %reshape.380), calls=%async_computation.2 | async-start | bytes 8192 | tf_op jit(solution)/shard_map/all_to_all | solution.py:124
  44.4 66.1 %reduce-scatter.2.cloned.1.call-start = ((), (), s32[]{:S(2)}) async-start(), calls=%async_computation.6 | async-start | bytes 163840 | tf_op jit(solution)/shard_map/reduce_scatter | solution.py:157
  45.0 23.3 %copy-start.5 = (f32[2048]{0:T(1024)S(1)}, f32[2048]{0:T(1024)}, u32[]{:S(2)}) copy-start(f32[2048]{0:T(1024)} %param.28) | copy-start | bytes 24580
  80.2 3.5 %copy-start.1 = (bf16[1,2048,1024]{2,1,0:T(8,128)(2,1)S(1)}, bf16[1,2048,1024]{2,1,0:T(8,128)(2,1)}, u32[]{:S(2)}) copy-start(bf16[1,2048,1024]{2,1,0:T(8,128)(2,1)} %param.36) | copy-start | bytes 12582916
  111.9 10.3 %all-to-all-start.4 = ((bf16[8,4,512]{2,1,0:T(4,128)(2,1)}), bf16[8,4,512]{2,1,0:T(4,128)(2,1)S(1)}, u32[]{:S(2)}, u32[]{:S(2)}) async-start(bf16[8,4,512]{2,1,0:T(4,128)(2,1)} %copy.70), calls=%async_computation.5 | async-start | bytes 65536 | tf_op jit(solution)/shard_map/all_to_all | solution.py:160
Sparse Core Ops, SparseCore 0:
  88.2 22.2 reduce-scatter.1
where the time goes:
time: 131 us; the launch traced here: 130 us
  blocking collectives  36.7 us (28%)
  waiting for transfers between devices  34.4 us (26%)
  matrix products  16.3 us (12%)
  starting transfers between devices  15.3 us (12%)
  between operations  15 us (11%)
  local copies, waits for them, and re-layouts  7.69 us (6%)
  other arithmetic  4.59 us (4%)
    reduce_scatter x1, waiting for transfers between devices, local(): lax.psum_scatter(partial_value.astype(jnp.bfloat16), 'tp', scatter_dimens...  22.2 us
    all_to_all x1, blocking collectives, local(): slots = lax.all_to_all(send, 'ep', split_axis=0, concat_axis=0, tiled=True)  11.4 us
    all_gather x1, blocking collectives, local(): gathered = lax.all_gather(resid, 'tp', axis=1, tiled=True)  9.93 us
    all_gather x1, blocking collectives, local(): updated_rows = lax.all_gather(updated, 'tp', axis=1, tiled=True)  8.12 us
    all_gather x1, blocking collectives, local(): lax.all_gather(mixed, 'tp', axis=0, tiled=True)  7.25 us
    all_to_all x1, waiting for transfers between devices, local(): lax.all_to_all(key_part, 'tp', split_axis=0, concat_axis=1, tiled=True)  4.63 us
    all_to_all x1, starting transfers between devices, local(): lax.all_to_all(summed.astype(jnp.bfloat16), 'ep', split_axis=0, concat_ax...  4.6 us
    all_to_all x1, waiting for transfers between devices, local(): lax.all_to_all(summed.astype(jnp.bfloat16), 'ep', split_axis=0, concat_ax...  4.51 us
  transfers between devices with their start and end apart: 5, of which 4 were waited for; matrix products, arithmetic and copies ran while one was open for 9% of the time, Pallas kernels for 0%

commit v1 on v0

--- a/solution.py
+++ b/solution.py
@@ -139,7 +139,12 @@
         lax.all_gather(mixed, "tp", axis=0, tiled=True), w_out, preferred_element_type=jnp.float32
     )
     updated = (resid.astype(jnp.float32) + attn_proj).astype(jnp.bfloat16)
-    updated_rows = lax.all_gather(updated, "tp", axis=1, tiled=True)
+    ring = [updated]
+    for hop in range(3):
+        ring.append(lax.ppermute(ring[-1], "tp", [(dev, (dev + 1) % 4) for dev in range(4)]))
+    updated_rows = jnp.roll(
+        jnp.concatenate(ring[::-1], axis=1), (lax.axis_index("tp") + 1) * ring[0].shape[1], axis=1
+    )
     hidden = scaled_rows(updated_rows, ffn_gain).astype(jnp.bfloat16)
     experts = w_gate.shape[0] * lax.axis_size("ep")
     dispatch, combine = route_tables(routes, route_weights, experts, CAP)

time: 131 us -> 136 us (1.038)
  waiting for transfers between devices: 34.4 us -> 45.4 us
  blocking collectives: 36.7 us -> 28.6 us
  starting transfers between devices: 15.3 us -> 17.3 us
    ppermute x0 -> x3, waiting for transfers between devices: none -> 11 us  [local(): lax.ppermute(ring[-1], 'tp', [(dev, (dev + 1) % 4) for dev in range(4)])]
    all_gather x1 -> x0, blocking collectives: 8.12 us -> none  [local(): updated_rows = lax.all_gather(updated, 'tp', axis=1, tiled=True)]
    ppermute x0 -> x3, starting transfers between devices: none -> 2.02 us  [local(): lax.ppermute(ring[-1], 'tp', [(dev, (dev + 1) % 4) for dev in range(4)])]
  transfers between devices with their start and end apart: 5 -> 8, of which waited for: 4 -> 7; matrix products, arithmetic and copies ran while one was open for 9% -> 8% of each run, Pallas kernels for 0% -> 0%
where the time goes in v1:
time: 136 us; the launch traced here: 135 us
  waiting for transfers between devices  45.4 us (33%)
  blocking collectives  28.6 us (21%)
  starting transfers between devices  17.3 us (13%)
  matrix products  16.3 us (12%)
  between operations  15 us (11%)
  local copies, waits for them, and re-layouts  7.78 us (6%)
  other arithmetic  4.58 us (3%)
    reduce_scatter x1, waiting for transfers between devices, local(): lax.psum_scatter(partial_value.astype(jnp.bfloat16), 'tp', scatter_dimens...  22.2 us
    all_to_all x1, blocking collectives, local(): slots = lax.all_to_all(send, 'ep', split_axis=0, concat_axis=0, tiled=True)  11.4 us
    ppermute x3, waiting for transfers between devices, local(): lax.ppermute(ring[-1], 'tp', [(dev, (dev + 1) % 4) for dev in range(4)])  11 us
    all_gather x1, blocking collectives, local(): gathered = lax.all_gather(resid, 'tp', axis=1, tiled=True)  9.93 us
    all_gather x1, blocking collectives, local(): lax.all_gather(mixed, 'tp', axis=0, tiled=True)  7.25 us
    all_to_all x1, waiting for transfers between devices, local(): lax.all_to_all(key_part, 'tp', split_axis=0, concat_axis=1, tiled=True)  4.63 us
    all_to_all x1, starting transfers between devices, local(): lax.all_to_all(summed.astype(jnp.bfloat16), 'ep', split_axis=0, concat_ax...  4.6 us
    all_to_all x1, waiting for transfers between devices, local(): lax.all_to_all(summed.astype(jnp.bfloat16), 'ep', split_axis=0, concat_ax...  4.51 us
  transfers between devices with their start and end apart: 8, of which 7 were waited for; matrix products, arithmetic and copies ran while one was open for 8% of the time, Pallas kernels for 0%

profile of v1, /device:TPU:0, one launch (start us, length us, event | category | flops | bytes accessed | tf_op | source)
XLA Modules:
  0.0 134.9 jit_solution(3933955574215006943)
XLA Ops:
  7.2 9.9 %all_gather.6 = bf16[4,2048]{1,0:T(4,128)(2,1)S(1)} all-gather(bf16[4,512]{1,0:T(4,128)(2,1)} %param.19), channel_id=1, replica_groups=mesh['ep'=8,'tp'=4] {'tp'}, dimensions={1}, use_global_device_ids=true | all-gather | bytes 20480 | tf_op jit(solution)/shard_map/all_gather | solution.py:116
  17.3 1.1 fusion.18
  20.2 3.2 %all-to-all-start = ((bf16[4,2,256]{2,1,0:T(2,128)(2,1)}), bf16[4,2,256]{2,1,0:T(2,128)(2,1)S(1)}, u32[]{:S(2)}, u32[]{:S(2)}) async-start(bf16[4,2,256]{2,1,0:T(2,128)(2,1)} %reshape.382), calls=%async_computation | async-start | bytes 8192 | tf_op jit(solution)/shard_map/all_to_all | solution.py:122
  23.7 2.1 %fusion.19 = bf16[4,1,512]{2,0,1:T(4,128)(2,1)S(1)} fusion(bf16[2048,512]{1,0:T(8,128)(2,1)} %param.30, bf16[4,2048]{1,0:T(4,128)(2,1)S(1)} %all_gather.6, f32[2048]{0:T(1024)S(1)} %copy-done.3, f32[4]{0:T(128)S(1)} %add_rsqrt_fusion.4), kind=kOutput, calls=%fused_computation.19 | convolution fusion | flops 8423424 | bytes 2125840 | tf_op jit(solution)/shard_map/dot_general | solution.py:119
  28.3 2.2 %reshape.356 = bf16[8,224,2,128]{3,2,1,0:T(2,128)(2,1)S(1)} reshape(bf16[1,8,224,256]{3,2,1,0:T(8,128)(2,1)} %param.20) | data formatting | bytes 1835008 | tf_op jit(solution)/shard_map/reshape.7
  31.8 4.2 %all-to-all-start.1 = ((bf16[4,2,256]{2,1,0:T(2,128)(2,1)}), bf16[4,2,256]{2,1,0:T(2,128)(2,1)S(1)}, u32[]{:S(2)}, u32[]{:S(2)}) async-start(bf16[4,2,256]{2,1,0:T(2,128)(2,1)} %reshape.384), calls=%async_computation.1 | async-start | bytes 8192 | tf_op jit(solution)/shard_map/all_to_all | solution.py:123
  36.0 4.6 %all-to-all-done.1 = bf16[4,2,256]{2,1,0:T(2,128)(2,1)S(1)} async-done(((bf16[4,2,256]{2,1,0:T(2,128)(2,1)}), bf16[4,2,256]{2,1,0:T(2,128)(2,1)S(1)}, u32[]{:S(2)}, u32[]{:S(2)}) %all-to-all-start.1) | async-done | bytes 4128 | tf_op jit(solution)/shard_map/all_to_all | solution.py:123
  40.6 3.2 %all-to-all-start.2 = ((bf16[4,2,256]{2,1,0:T(2,128)(2,1)}), bf16[4,2,256]{2,1,0:T(2,128)(2,1)S(1)}, u32[]{:S(2)}, u32[]{:S(2)}) async-start(bf16[4,2,256]{2,1,0:T(2,128)(2,1)} %reshape.380), calls=%async_computation.2 | async-start | bytes 8192 | tf_op jit(solution)/shard_map/all_to_all | solution.py:124
  45.5 3.0 %all-to-all-done.2 = bf16[4,2,256]{2,1,0:T(2,128)(2,1)S(1)} async-done(((bf16[4,2,256]{2,1,0:T(2,128)(2,1)}), bf16[4,2,256]{2,1,0:T(2,128)(2,1)S(1)}, u32[]{:S(2)}, u32[]{:S(2)}) %all-to-all-start.2) | async-done | bytes 4128 | tf_op jit(solution)/shard_map/all_to_all | solution.py:124
  48.6 1.4 %fusion.21 = f32[8,1,256]{2,1,0:T(1,128)S(1)} fusion(bf16[1,8,224,256]{3,2,1,0:T(8,128)(2,1)} %param.21, bf16[8,224,1]{1,0,2:T(8,128)(2,1)S(1)} %fusion.50), kind=kOutput, calls=%fused_computation.21 | convolution fusion | flops 917504 | bytes 929280 | tf_op jit(solution)/shard_map/sjgl,sjlv->sjgv/dot_general | solution.py:80
  50.3 7.2 %all-gather = bf16[4,1,2048]{2,1,0:T(2,128)(2,1)S(1)} all-gather(bf16[1,1,2048]{2,1,0:T(2,128)(2,1)S(1)} %reshape.365), channel_id=1, replica_groups=mesh['ep'=8,'tp'=4] {'tp'}, dimensions={0}, use_global_device_ids=true | all-gather | bytes 20480 | tf_op jit(solution)/shard_map/all_gather | solution.py:139
  57.6 2.0 %fusion.15 = bf16[4,512]{1,0:T(4,128)(2,1)S(1)} fusion(bf16[2048,512]{1,0:T(8,128)(2,1)} %param.32, bf16[4,1,2048]{2,1,0:T(2,128)(2,1)S(1)} %all-gather, bf16[4,512]{1,0:T(4,128)(2,1)S(1)} %copy-done.4), kind=kOutput, calls=%fused_computation.12 | convolution fusion | flops 8394752 | bytes 2121728 | tf_op jit(solution)/shard_map/dot_general | solution.py:138
  59.5 1.5 %collective-permute-start = (bf16[4,512]{1,0:T(4,128)(2,1)S(1)}, bf16[4,512]{1,0:T(4,128)(2,1)S(1)}, u32[]{:S(2)}, u32[]{:S(2)}) collective-permute-start(bf16[4,512]{1,0:T(4,128)(2,1)S(1)} %fusion.15), channel_id=1, source_target_pairs={{0,1},{1,2},{2,3},{3,0},{4,5},{5,6},{6,7},{7,4},{8,9},{9,10},{10,1... | collective-permute-start | bytes 12296 | tf_op jit(solution)/shard_map/ppermute | solution.py:144
  61.3 2.8 %collective-permute-done = bf16[4,512]{1,0:T(4,128)(2,1)S(1)} collective-permute-done((bf16[4,512]{1,0:T(4,128)(2,1)S(1)}, bf16[4,512]{1,0:T(4,128)(2,1)S(1)}, u32[]{:S(2)}, u32[]{:S(2)}) %collective-permute-start) | collective-permute-done | bytes 4128 | tf_op jit(solution)/shard_map/ppermute | solution.py:144
  64.8 3.8 %collective-permute-done.1 = bf16[4,512]{1,0:T(4,128)(2,1)S(1)} collective-permute-done((bf16[4,512]{1,0:T(4,128)(2,1)S(1)}, bf16[4,512]{1,0:T(4,128)(2,1)S(1)}, u32[]{:S(2)}, u32[]{:S(2)}) %collective-permute-start.1) | collective-permute-done | bytes 4128 | tf_op jit(solution)/shard_map/ppermute | solution.py:144
  68.7 4.4 %collective-permute-done.2 = bf16[4,512]{1,0:T(4,128)(2,1)S(1)} collective-permute-done((bf16[4,512]{1,0:T(4,128)(2,1)S(1)}, bf16[4,512]{1,0:T(4,128)(2,1)S(1)}, u32[]{:S(2)}, u32[]{:S(2)}) %collective-permute-start.2) | collective-permute-done | bytes 4128 | tf_op jit(solution)/shard_map/ppermute | solution.py:144
  73.7 11.4 %all_to_all.49 = bf16[8,4,2048]{2,1,0:T(4,128)(2,1)S(1)} all-to-all(bf16[8,4,2048]{2,1,0:T(4,128)(2,1)S(1)} %copy.68), channel_id=1, replica_groups=mesh['ep'=8,'tp'=4] {'ep'}, dimensions={0} | all-to-all | bytes 262144 | tf_op jit(solution)/shard_map/all_to_all | solution.py:154
  85.2 3.2 %fusion.4 = f32[32,1024]{1,0:T(8,128)S(1)} fusion(bf16[32,2048]{1,0:T(8,128)(2,1)S(1)} %reshape.359, bf16[1,2048,1024]{2,1,0:T(8,128)(2,1)} %param.35), kind=kOutput, calls=%fused_computation.4 | convolution fusion | flops 134217728 | bytes 4456448 | tf_op jit(solution)/shard_map/dot_general | solution.py:156
  89.5 3.6 %fusion.6 = bf16[8,4,2048]{2,0,1:T(8,128)(2,1)} fusion(bf16[1,1024,2048]{2,1,0:T(8,128)(2,1)} %param.37, bf16[8,4,1024]{2,1,0:T(4,128)(2,1)S(1)} %dot_general.48), kind=kOutput, calls=%fused_computation.6 | convolution fusion | flops 134283264 | bytes 4390912 | tf_op jit(solution)/shard_map/dot_general | solution.py:159
  93.3 22.2 %reduce-scatter.2.cloned.1.call-done = bf16[8,4,512]{2,0,1:T(8,128)(2,1)} async-done(((bf16[8,4,2048]{2,0,1:T(8,128)(2,1)}), bf16[8,4,512]{2,0,1:T(8,128)(2,1)}) %reduce-scatter.2.cloned.1.call-update) | async-done | bytes 32784 | tf_op jit(solution)/shard_map/reduce_scatter | solution.py:162
  115.5 1.4 %copy.70 = bf16[8,4,512]{2,1,0:T(4,128)(2,1)} copy(bf16[8,4,512]{2,0,1:T(8,128)(2,1)} %reduce-scatter.2.cloned.1.call-done) | data formatting | bytes 65536 | tf_op jit(solution)/shard_map/reduce_scatter | solution.py:162
  116.9 4.6 %all-to-all-start.4 = ((bf16[8,4,512]{2,1,0:T(4,128)(2,1)}), bf16[8,4,512]{2,1,0:T(4,128)(2,1)S(1)}, u32[]{:S(2)}, u32[]{:S(2)}) async-start(bf16[8,4,512]{2,1,0:T(4,128)(2,1)} %copy.70), calls=%async_computation.5 | async-start | bytes 65536 | tf_op jit(solution)/shard_map/all_to_all | solution.py:165
  122.7 4.5 %all-to-all-done.4 = bf16[8,4,512]{2,1,0:T(4,128)(2,1)S(1)} async-done(((bf16[8,4,512]{2,1,0:T(4,128)(2,1)}), bf16[8,4,512]{2,1,0:T(4,128)(2,1)S(1)}, u32[]{:S(2)}, u32[]{:S(2)}) %all-to-all-start.4) | async-done | bytes 32800 | tf_op jit(solution)/shard_map/all_to_all | solution.py:165
  127.2 0.8 fusion.17
  (99 shorter events, 11.5 us)
Async XLA Ops:
  7.2 10.1 %copy-start = (bf16[2048,512]{1,0:T(8,128)(2,1)S(1)}, bf16[2048,512]{1,0:T(8,128)(2,1)}, u32[]{:S(2)}) copy-start(bf16[2048,512]{1,0:T(8,128)(2,1)} %param.29) | copy-start | bytes 6291460
  7.2 16.5 %copy-start.3 = (f32[2048]{0:T(1024)S(1)}, f32[2048]{0:T(1024)}, u32[]{:S(2)}) copy-start(f32[2048]{0:T(1024)} %param.24) | copy-start | bytes 24580
  7.2 16.2 %copy-start.7 = (s32[4,2]{0,1:T(2,128)S(1)}, s32[4,2]{0,1:T(2,128)}, u32[]{:S(2)}) copy-start(s32[4,2]{0,1:T(2,128)} %param.33) | copy-start | bytes 100
  20.2 11.6 %all-to-all-start = ((bf16[4,2,256]{2,1,0:T(2,128)(2,1)}), bf16[4,2,256]{2,1,0:T(2,128)(2,1)S(1)}, u32[]{:S(2)}, u32[]{:S(2)}) async-start(bf16[4,2,256]{2,1,0:T(2,128)(2,1)} %reshape.382), calls=%async_computation | async-start | bytes 8192 | tf_op jit(solution)/shard_map/all_to_all | solution.py:122
  23.6 2.9 %copy-start.2 = (bf16[2048,512]{1,0:T(8,128)(2,1)S(1)}, bf16[2048,512]{1,0:T(8,128)(2,1)}, u32[]{:S(2)}) copy-start(bf16[2048,512]{1,0:T(8,128)(2,1)} %param.31) | copy-start | bytes 6291460
  25.8 18.4 %copy-start.10 = (f32[128]{0:T(128)S(1)}, f32[128]{0:T(128)}, u32[]{:S(2)}) copy-start(f32[128]{0:T(128)} %param.25) | copy-start | bytes 1540
  25.8 18.4 %copy-start.11 = (f32[128]{0:T(128)S(1)}, f32[128]{0:T(128)}, u32[]{:S(2)}) copy-start(f32[128]{0:T(128)} %param.26) | copy-start | bytes 1540
  26.5 18.9 %copy-start.6 = (f32[8]{0:T(128)S(1)}, f32[8]{0:T(128)}, u32[]{:S(2)}) copy-start(f32[8]{0:T(128)} %param.23) | copy-start | bytes 100
  27.0 23.2 %copy-start.8 = (f32[256]{0:T(256)S(1)}, f32[256]{0:T(256)}, u32[]{:S(2)}) copy-start(f32[256]{0:T(256)} %param.27) | copy-start | bytes 3076
  28.3 29.2 %copy-start.4 = (bf16[4,512]{1,0:T(4,128)(2,1)S(1)}, bf16[4,512]{1,0:T(4,128)(2,1)}, u32[]{:S(2)}) copy-start(bf16[4,512]{1,0:T(4,128)(2,1)} %param.19) | copy-start | bytes 12292
  31.8 8.8 %all-to-all-start.1 = ((bf16[4,2,256]{2,1,0:T(2,128)(2,1)}), bf16[4,2,256]{2,1,0:T(2,128)(2,1)S(1)}, u32[]{:S(2)}, u32[]{:S(2)}) async-start(bf16[4,2,256]{2,1,0:T(2,128)(2,1)} %reshape.384), calls=%async_computation.1 | async-start | bytes 8192 | tf_op jit(solution)/shard_map/all_to_all | solution.py:123
  40.6 7.9 %all-to-all-start.2 = ((bf16[4,2,256]{2,1,0:T(2,128)(2,1)}), bf16[4,2,256]{2,1,0:T(2,128)(2,1)S(1)}, u32[]{:S(2)}, u32[]{:S(2)}) async-start(bf16[4,2,256]{2,1,0:T(2,128)(2,1)} %reshape.380), calls=%async_computation.2 | async-start | bytes 8192 | tf_op jit(solution)/shard_map/all_to_all | solution.py:124
  43.9 71.6 %reduce-scatter.2.cloned.1.call-start = ((), (), s32[]{:S(2)}) async-start(), calls=%async_computation.6 | async-start | bytes 163840 | tf_op jit(solution)/shard_map/reduce_scatter | solution.py:162
  44.5 20.2 %copy-start.9 = (f32[4,2]{0,1:T(2,128)S(1)}, f32[4,2]{0,1:T(2,128)}, u32[]{:S(2)}) copy-start(f32[4,2]{0,1:T(2,128)} %param.34) | copy-start | bytes 100
  44.5 28.8 %copy-start.5 = (f32[2048]{0:T(1024)S(1)}, f32[2048]{0:T(1024)}, u32[]{:S(2)}) copy-start(f32[2048]{0:T(1024)} %param.28) | copy-start | bytes 24580
  59.5 4.5 %collective-permute-start = (bf16[4,512]{1,0:T(4,128)(2,1)S(1)}, bf16[4,512]{1,0:T(4,128)(2,1)S(1)}, u32[]{:S(2)}, u32[]{:S(2)}) collective-permute-start(bf16[4,512]{1,0:T(4,128)(2,1)S(1)} %fusion.15), channel_id=1, source_target_pairs={{0,1},{1,2},{2,3},{3,0},{4,5},{5,6},{6,7},{7,4},{8,9},{9,10},{10,1... | collective-permute-start | bytes 12296 | tf_op jit(solution)/shard_map/ppermute | solution.py:144
  64.1 4.5 %collective-permute-start.1 = (bf16[4,512]{1,0:T(4,128)(2,1)S(1)}, bf16[4,512]{1,0:T(4,128)(2,1)S(1)}, u32[]{:S(2)}, u32[]{:S(2)}) collective-permute-start(bf16[4,512]{1,0:T(4,128)(2,1)S(1)} %collective-permute-done), channel_id=1, source_target_pairs={{0,1},{1,2},{2,3},{3,0},{4,5},{5,6},{6,7},{7,4},{8,9},{9,10},{10,1... | collective-permute-start | bytes 12296 | tf_op jit(solution)/shard_map/ppermute | solution.py:144
  68.6 4.5 %collective-permute-start.2 = (bf16[4,512]{1,0:T(4,128)(2,1)S(1)}, bf16[4,512]{1,0:T(4,128)(2,1)S(1)}, u32[]{:S(2)}, u32[]{:S(2)}) collective-permute-start(bf16[4,512]{1,0:T(4,128)(2,1)S(1)} %collective-permute-done.1), channel_id=1, source_target_pairs={{0,1},{1,2},{2,3},{3,0},{4,5},{5,6},{6,7},{7,4},{8,9},{9,10},{10,1... | collective-permute-start | bytes 12296 | tf_op jit(solution)/shard_map/ppermute | solution.py:144
  85.1 3.5 %copy-start.1 = (bf16[1,2048,1024]{2,1,0:T(8,128)(2,1)S(1)}, bf16[1,2048,1024]{2,1,0:T(8,128)(2,1)}, u32[]{:S(2)}) copy-start(bf16[1,2048,1024]{2,1,0:T(8,128)(2,1)} %param.36) | copy-start | bytes 12582916
  116.9 10.3 %all-to-all-start.4 = ((bf16[8,4,512]{2,1,0:T(4,128)(2,1)}), bf16[8,4,512]{2,1,0:T(4,128)(2,1)S(1)}, u32[]{:S(2)}, u32[]{:S(2)}) async-start(bf16[8,4,512]{2,1,0:T(4,128)(2,1)} %copy.70), calls=%async_computation.5 | async-start | bytes 65536 | tf_op jit(solution)/shard_map/all_to_all | solution.py:165
Sparse Core Ops, SparseCore 0:
  93.2 22.2 reduce-scatter.1
